TPU v7x, 512 devices: a whole 4x8x8 slice. The times are simulated.
512 devices in a mesh: kv: 64 (over z, y), tp: 8 (over x, core).
Axes of the slice: x: 4, y: 8, z: 8, core: 2. Of those that a mesh axis runs over, the one named last changes fastest.
Arguments:
- hidden_in: bfloat16 [1024, 2048], P('kv', 'tp'), may hold values from -6 to 6
- first_gain: bfloat16 [2048], P('tp'), may hold values from 0.099609375 to 1.8984375
- first_gate_proj: bfloat16 [2048, 5632], P('tp', 'kv'), may hold values from -0.125 to 0.125
- first_up_proj: bfloat16 [2048, 5632], P('tp', 'kv'), may hold values from -0.125 to 0.125
- first_down_proj: bfloat16 [5632, 2048], P('kv', 'tp'), may hold values from -0.078125 to 0.078125
- mix_gain: bfloat16 [2048], replicated, may hold values from 0.099609375 to 1.8984375
- query_weight: bfloat16 [2048, 1024], P(None, 'tp'), may hold values from -0.125 to 0.125
- forget_weight: bfloat16 [2048, 1024], P(None, 'tp'), may hold values from -0.125 to 0.125
- input_weight: bfloat16 [2048, 1024], P(None, 'tp'), may hold values from -0.125 to 0.125
- outgate_weight: bfloat16 [2048, 1024], P(None, 'tp'), may hold values from -0.125 to 0.125
- forget_floor: float32 [1024], P('tp'), may hold values from 0.05 to 0.95
- state_in: float32 [1024, 8, 128, 128], P('kv', 'tp'), may hold values from -6 to 6
- out_gain: bfloat16 [1024], P('tp'), may hold values from 0.099609375 to 1.8984375
- mix_out_weight: bfloat16 [1024, 2048], P('tp'), may hold values from -0.1875 to 0.1875
- second_gain: bfloat16 [2048], P('tp'), may hold values from 0.099609375 to 1.8984375
- second_gate_proj: bfloat16 [2048, 5632], P('tp', 'kv'), may hold values from -0.125 to 0.125
- second_up_proj: bfloat16 [2048, 5632], P('tp', 'kv'), may hold values from -0.125 to 0.125
- second_down_proj: bfloat16 [5632, 2048], P('kv', 'tp'), may hold values from -0.078125 to 0.078125
Outputs:
- hidden_out: bfloat16 [1024, 2048], P('kv', 'tp')
- state_out: float32 [1024, 8, 128, 128], P('kv', 'tp')
All inputs are finite; a program needn't handle non-finite values.
Results may differ from a plain program's by a relative error of at most 0.019.
Values may be sent and summed in bfloat16 or wider, within the bound.
A program may use at most 64 MiB of HBM per device.

v0:
```python
import jax
import jax.numpy as jnp
from jax import lax
from jax.sharding import PartitionSpec as P

D = 2048


def sent_to_all(shard, axis):
    copies = jnp.broadcast_to(shard, (lax.axis_size(axis), *shard.shape))
    return lax.all_to_all(copies, axis, split_axis=0, concat_axis=0, tiled=True)


def joined_along(blocks, dim):
    shape = list(blocks.shape[1:])
    shape[dim] *= blocks.shape[0]
    return jnp.moveaxis(blocks, 0, dim).reshape(shape)


def collect(shard, axis, dim):
    blocks = sent_to_all(shard, axis)
    return joined_along(blocks, dim)


def taken_together(shard, axis):
    return sent_to_all(shard, axis).astype(jnp.float32).sum(axis=0)


def split_up(shard, dim, count):
    before, after = (shard.shape[:dim], shard.shape[dim + 1 :])
    return jnp.moveaxis(shard.reshape(*before, count, -1, *after), dim, 0)


def sum_at_owner(shard, axis, dim):
    count = lax.axis_size(axis)
    blocks = lax.all_to_all(split_up(shard, dim, count), axis, 0, 0, tiled=True)
    return jnp.sum(blocks.astype(jnp.float32), axis=0)


def feed_forward(hidden, norm_gain, gate_proj, up_proj, down_proj):
    gathered = collect(hidden, "kv", 0)
    values = gathered.astype(jnp.float32)
    square_part = jnp.sum(values * values, axis=1)
    scaled = (values * norm_gain.astype(jnp.float32)).astype(jnp.bfloat16)
    gate_part = jnp.dot(scaled, gate_proj, preferred_element_type=jnp.float32)
    up_part = jnp.dot(scaled, up_proj, preferred_element_type=jnp.float32)
    gate_sum, up_sum, square_sum = (
        taken_together(gate_part.astype(jnp.bfloat16), "tp").astype(jnp.float32),
        taken_together(up_part.astype(jnp.bfloat16), "tp").astype(jnp.float32),
        taken_together(square_part.astype(jnp.bfloat16), "tp").astype(jnp.float32),
    )
    inverse = lax.rsqrt(square_sum / D + 1e-06)[:, None]
    inner_units = (jax.nn.silu(gate_sum * inverse) * (up_sum * inverse)).astype(jnp.bfloat16)
    own_units = lax.all_to_all(inner_units, "kv", split_axis=0, concat_axis=1, tiled=True)
    down_sum = jnp.dot(
        own_units,
        lax.all_gather(down_proj, "kv", axis=0, tiled=True),
        preferred_element_type=jnp.float32,
    )
    return (hidden.astype(jnp.float32) + 0.5 * down_sum).astype(jnp.bfloat16)


def shards(
    hidden_in,
    first_gain,
    first_gate_proj,
    first_up_proj,
    first_down_proj,
    mix_gain,
    query_weight,
    forget_weight,
    input_weight,
    outgate_weight,
    forget_floor,
    state_in,
    out_gain,
    mix_out_weight,
    second_gain,
    second_gate_proj,
    second_up_proj,
    second_down_proj,
):
    first_out = feed_forward(hidden_in, first_gain, first_gate_proj, first_up_proj, first_down_proj)
    whole_rows = collect(first_out, "tp", 1)
    values = whole_rows.astype(jnp.float32)
    inverse = lax.rsqrt(jnp.mean(values * values, axis=1, keepdims=True) + 1e-06)
    normed = (values * inverse * mix_gain.astype(jnp.float32)).astype(jnp.bfloat16)
    batch_here = state_in.shape[0]
    heads_here = state_in.shape[1]
    head_size = state_in.shape[2]

    def project(weight):
        return jnp.dot(normed, weight, preferred_element_type=jnp.float32).reshape(
            batch_here, heads_here, head_size
        )

    query_vals = jax.nn.silu(project(query_weight))
    forget_pre = project(forget_weight)
    input_vals = project(input_weight)
    out_gate = project(outgate_weight)
    floor_vals = forget_floor.reshape(heads_here, head_size)
    log_forget = jnp.logaddexp(
        jnp.log(floor_vals), jnp.log1p(-floor_vals) + jax.nn.log_sigmoid(forget_pre)
    )
    key_vals = -jnp.expm1(log_forget)
    new_state = (
        jnp.exp(log_forget)[..., None] * state_in + key_vals[..., None] * input_vals[:, :, None, :]
    )
    readout = jnp.einsum("bhk,bhkv->bhv", query_vals, new_state, precision=lax.Precision.HIGHEST)
    normed_out = (
        readout
        * lax.rsqrt(jnp.mean(readout * readout, axis=-1, keepdims=True) + 1e-05)
        * out_gain.astype(jnp.float32).reshape(heads_here, head_size)
    )
    gated_out = (
        (normed_out * jax.nn.silu(out_gate))
        .reshape(batch_here, heads_here * head_size)
        .astype(jnp.bfloat16)
    )
    partial_value = jnp.dot(gated_out, mix_out_weight, preferred_element_type=jnp.float32)
    mixed_sum = sum_at_owner(partial_value.astype(jnp.bfloat16), "tp", 1)
    second_in = (first_out.astype(jnp.float32) + mixed_sum).astype(jnp.bfloat16)
    hidden_out = feed_forward(
        second_in, second_gain, second_gate_proj, second_up_proj, second_down_proj
    )
    return (hidden_out, new_state)


def solution(mesh):
    placed = (
        P("kv", "tp"),
        P("tp"),
        P("tp", "kv"),
        P("tp", "kv"),
        P("kv", "tp"),
        P(),
        P(None, "tp"),
        P(None, "tp"),
        P(None, "tp"),
        P(None, "tp"),
        P("tp"),
        P("kv", "tp", None, None),
        P("tp"),
        P("tp", None),
        P("tp"),
        P("tp", "kv"),
        P("tp", "kv"),
        P("kv", "tp"),
    )
    return jax.shard_map(
        shards,
        mesh=mesh,
        in_specs=placed,
        out_specs=(P("kv", "tp"), P("kv", "tp", None, None)),
        check_vma=False,
    )
```

profile of v0, /device:TPU:1, one launch (start us, length us, event | category | flops | bytes accessed | tf_op | source)
XLA Modules:
  0.0 267.9 jit_solution(9169292357920632488)
XLA Ops:
  7.2 0.7 all-gather.3.cloned.1.call-update
  7.9 1.5 broadcast_in_dim.18
  9.4 17.1 %all-to-all-start = ((bf16[64,16,256]{2,1,0:T(8,128)(2,1)}), bf16[64,16,256]{2,1,0:T(8,128)(2,1)S(1)}, u32[]{:S(2)}, u32[]{:S(2)}) async-start(bf16[64,16,256]{2,1,0:T(8,128)(2,1)} %broadcast_in_dim.18), calls=%async_computation | async-start | bytes 1048576 | tf_op jit(solution)/shard_map/all_to_all | solution.py:11
  26.6 0.7 convert_element_type.134
  27.2 16.5 %all-to-all-done = bf16[64,16,256]{2,1,0:T(8,128)(2,1)S(1)} async-done(((bf16[64,16,256]{2,1,0:T(8,128)(2,1)}), bf16[64,16,256]{2,1,0:T(8,128)(2,1)S(1)}, u32[]{:S(2)}, u32[]{:S(2)}) %all-to-all-start) | async-done | bytes 524320 | tf_op jit(solution)/shard_map/all_to_all | solution.py:11
  44.1 0.5 broadcast.151
  44.7 0.7 reduce.8
  45.4 0.6 reshape.192
  46.0 8.1 %all-to-all-start.2 = ((bf16[8,2,512]{2,1,0:T(2,128)(2,1)}), bf16[8,2,512]{2,1,0:T(2,128)(2,1)S(1)}, u32[]{:S(2)}, u32[]{:S(2)}) async-start(bf16[8,2,512]{2,1,0:T(2,128)(2,1)} %reshape.192), calls=%async_computation.2 | async-start | bytes 32768 | tf_op jit(solution)/shard_map/all_to_all | solution.py:11
  54.6 4.3 %all-to-all-done.2 = bf16[8,2,512]{2,1,0:T(2,128)(2,1)S(1)} async-done(((bf16[8,2,512]{2,1,0:T(2,128)(2,1)}), bf16[8,2,512]{2,1,0:T(2,128)(2,1)S(1)}, u32[]{:S(2)}, u32[]{:S(2)}) %all-to-all-start.2) | async-done | bytes 16416 | tf_op jit(solution)/shard_map/all_to_all | solution.py:11
  58.9 1.3 broadcast_in_dim.19
  60.2 4.1 %all-to-all-start.1 = ((bf16[8,1024,88]{1,2,0:T(8,128)(2,1)}), bf16[8,1024,88]{1,2,0:T(8,128)(2,1)S(1)}, u32[]{:S(2)}, u32[]{:S(2)}) async-start(bf16[8,1024,88]{1,2,0:T(8,128)(2,1)} %broadcast_in_dim.19), calls=%async_computation.1 | async-start | bytes 2883584 | tf_op jit(solution)/shard_map/all_to_all | solution.py:11
  64.6 18.9 %all-to-all-done.1 = bf16[8,1024,88]{1,2,0:T(8,128)(2,1)S(1)} async-done(((bf16[8,1024,88]{1,2,0:T(8,128)(2,1)}), bf16[8,1024,88]{1,2,0:T(8,128)(2,1)S(1)}, u32[]{:S(2)}, u32[]{:S(2)}) %all-to-all-start.1) | async-done | bytes 1441824 | tf_op jit(solution)/shard_map/all_to_all | solution.py:11
  83.5 1.3 broadcast_in_dim.41
  84.8 4.4 %all-to-all-start.3 = ((bf16[8,1024,88]{1,2,0:T(8,128)(2,1)}), bf16[8,1024,88]{1,2,0:T(8,128)(2,1)S(1)}, u32[]{:S(2)}, u32[]{:S(2)}) async-start(bf16[8,1024,88]{1,2,0:T(8,128)(2,1)} %broadcast_in_dim.41), calls=%async_computation.3 | async-start | bytes 2883584 | tf_op jit(solution)/shard_map/all_to_all | solution.py:11
  89.4 1.0 convert_reduce_fusion.3
  90.4 1.2 copy.66
  91.6 16.9 %all-to-all-done.3 = bf16[8,1024,88]{1,2,0:T(8,128)(2,1)S(1)} async-done(((bf16[8,1024,88]{1,2,0:T(8,128)(2,1)}), bf16[8,1024,88]{1,2,0:T(8,128)(2,1)S(1)}, u32[]{:S(2)}, u32[]{:S(2)}) %all-to-all-start.3) | async-done | bytes 1441824 | tf_op jit(solution)/shard_map/all_to_all | solution.py:11
  109.0 0.9 multiply_convert_fusion.1
  109.9 4.9 %all-to-all-start.4 = ((bf16[64,16,88]{2,1,0:T(8,128)(2,1)}), bf16[64,16,88]{2,1,0:T(8,128)(2,1)S(1)}, u32[]{:S(2)}, u32[]{:S(2)}) async-start(bf16[64,16,88]{2,1,0:T(8,128)(2,1)} %multiply_convert_fusion.1), calls=%async_computation.4 | async-start | bytes 524288 | tf_op jit(solution)/shard_map/all_to_all | solution.py:54
  114.9 0.7 all-gather.5.cloned.1.call-update
  115.6 11.9 %all-to-all-done.4 = bf16[64,16,88]{2,1,0:T(8,128)(2,1)S(1)} async-done(((bf16[64,16,88]{2,1,0:T(8,128)(2,1)}), bf16[64,16,88]{2,1,0:T(8,128)(2,1)S(1)}, u32[]{:S(2)}, u32[]{:S(2)}) %all-to-all-start.4) | async-done | bytes 180256 | tf_op jit(solution)/shard_map/all_to_all | solution.py:54
  128.0 2.4 fusion.2
  130.4 0.6 broadcast_in_dim.42
  131.0 6.4 %all-to-all-start.5 = ((bf16[8,16,256]{2,1,0:T(8,128)(2,1)}), bf16[8,16,256]{2,1,0:T(8,128)(2,1)S(1)}, u32[]{:S(2)}, u32[]{:S(2)}) async-start(bf16[8,16,256]{2,1,0:T(8,128)(2,1)} %broadcast_in_dim.42), calls=%async_computation.5 | async-start | bytes 131072 | tf_op jit(solution)/shard_map/all_to_all | solution.py:11
  137.5 4.8 %all-to-all-done.5 = bf16[8,16,256]{2,1,0:T(8,128)(2,1)S(1)} async-done(((bf16[8,16,256]{2,1,0:T(8,128)(2,1)}), bf16[8,16,256]{2,1,0:T(8,128)(2,1)S(1)}, u32[]{:S(2)}, u32[]{:S(2)}) %all-to-all-start.5) | async-done | bytes 65568 | tf_op jit(solution)/shard_map/all_to_all | solution.py:11
  143.3 0.6 multiply_add_fusion
  143.9 1.0 copy-done.1
  144.8 1.0 fusion.5
  146.0 0.4 convolution_convert_fusion
  146.3 8.0 %all_to_all.84 = bf16[8,16,256]{2,1,0:T(8,128)(2,1)S(1)} all-to-all(bf16[8,16,256]{2,1,0:T(8,128)(2,1)S(1)} %bitcast.62), channel_id=1, replica_groups=mesh['kv'=64,'tp'=8] {'tp'}, dimensions={0} | all-to-all | bytes 131072 | tf_op jit(solution)/shard_map/all_to_all | solution.py:36
  154.4 0.8 broadcast_in_dim.43
  155.2 4.6 %all-to-all-start.7 = ((bf16[64,16,256]{2,1,0:T(8,128)(2,1)}), bf16[64,16,256]{2,1,0:T(8,128)(2,1)S(1)}, u32[]{:S(2)}, u32[]{:S(2)}) async-start(bf16[64,16,256]{2,1,0:T(8,128)(2,1)} %broadcast_in_dim.43), calls=%async_computation.7 | async-start | bytes 1048576 | tf_op jit(solution)/shard_map/all_to_all | solution.py:11
  159.9 17.5 %all-to-all-done.7 = bf16[64,16,256]{2,1,0:T(8,128)(2,1)S(1)} async-done(((bf16[64,16,256]{2,1,0:T(8,128)(2,1)}), bf16[64,16,256]{2,1,0:T(8,128)(2,1)S(1)}, u32[]{:S(2)}, u32[]{:S(2)}) %all-to-all-start.7) | async-done | bytes 524320 | tf_op jit(solution)/shard_map/all_to_all | solution.py:11
  177.7 0.7 reduce.9
  178.5 0.6 reshape.194
  179.1 6.3 %all-to-all-start.9 = ((bf16[8,2,512]{2,1,0:T(2,128)(2,1)}), bf16[8,2,512]{2,1,0:T(2,128)(2,1)S(1)}, u32[]{:S(2)}, u32[]{:S(2)}) async-start(bf16[8,2,512]{2,1,0:T(2,128)(2,1)} %reshape.194), calls=%async_computation.9 | async-start | bytes 32768 | tf_op jit(solution)/shard_map/all_to_all | solution.py:11
  185.8 4.2 %all-to-all-done.9 = bf16[8,2,512]{2,1,0:T(2,128)(2,1)S(1)} async-done(((bf16[8,2,512]{2,1,0:T(2,128)(2,1)}), bf16[8,2,512]{2,1,0:T(2,128)(2,1)S(1)}, u32[]{:S(2)}, u32[]{:S(2)}) %all-to-all-start.9) | async-done | bytes 16416 | tf_op jit(solution)/shard_map/all_to_all | solution.py:11
  190.1 1.3 broadcast_in_dim.44
  191.4 4.2 %all-to-all-start.8 = ((bf16[8,1024,88]{1,2,0:T(8,128)(2,1)}), bf16[8,1024,88]{1,2,0:T(8,128)(2,1)S(1)}, u32[]{:S(2)}, u32[]{:S(2)}) async-start(bf16[8,1024,88]{1,2,0:T(8,128)(2,1)} %broadcast_in_dim.44), calls=%async_computation.8 | async-start | bytes 2883584 | tf_op jit(solution)/shard_map/all_to_all | solution.py:11
  195.9 18.9 %all-to-all-done.8 = bf16[8,1024,88]{1,2,0:T(8,128)(2,1)S(1)} async-done(((bf16[8,1024,88]{1,2,0:T(8,128)(2,1)}), bf16[8,1024,88]{1,2,0:T(8,128)(2,1)S(1)}, u32[]{:S(2)}, u32[]{:S(2)}) %all-to-all-start.8) | async-done | bytes 1441824 | tf_op jit(solution)/shard_map/all_to_all | solution.py:11
  214.8 1.3 broadcast_in_dim.46
  216.1 4.4 %all-to-all-start.10 = ((bf16[8,1024,88]{1,2,0:T(8,128)(2,1)}), bf16[8,1024,88]{1,2,0:T(8,128)(2,1)S(1)}, u32[]{:S(2)}, u32[]{:S(2)}) async-start(bf16[8,1024,88]{1,2,0:T(8,128)(2,1)} %broadcast_in_dim.46), calls=%async_computation.10 | async-start | bytes 2883584 | tf_op jit(solution)/shard_map/all_to_all | solution.py:11
  220.6 1.0 convert_reduce_fusion.1
  221.6 1.2 copy.72
  222.8 16.9 %all-to-all-done.10 = bf16[8,1024,88]{1,2,0:T(8,128)(2,1)S(1)} async-done(((bf16[8,1024,88]{1,2,0:T(8,128)(2,1)}), bf16[8,1024,88]{1,2,0:T(8,128)(2,1)S(1)}, u32[]{:S(2)}, u32[]{:S(2)}) %all-to-all-start.10) | async-done | bytes 1441824 | tf_op jit(solution)/shard_map/all_to_all | solution.py:11
  240.4 17.3 %all_to_all.85 = bf16[64,16,88]{2,1,0:T(8,128)(2,1)S(1)} all-to-all(bf16[64,16,88]{2,1,0:T(8,128)(2,1)S(1)} %multiply_convert_fusion), channel_id=1, replica_groups=mesh['kv'=64,'tp'=8] {'kv'}, dimensions={0} | all-to-all | bytes 360448 | tf_op jit(solution)/shard_map/all_to_all | solution.py:54
  258.2 2.9 %fusion.3 = bf16[16,256]{1,0:T(8,128)(2,1)} fusion(bf16[16,5632]{1,0:T(8,128)(2,1)S(1)} %all_to_all.71, bf16[5632,256]{1,0:T(8,128)(2,1)} %all-gather.5.cloned.1.call-done, bf16[16,256]{1,0:T(8,128)(2,1)S(1)} %add_convert_fusion), kind=kOutput, calls=%fused_computation.14 | convolution fusion | flops 46153728 | bytes 3080192 | tf_op jit(solution)/shard_map/dot_general | solution.py:55
  (81 shorter events, 5.4 us)
Async XLA Ops:
  7.2 138.8 %copy-start = (bf16[128,2048]{1,0:T(8,128)(2,1)S(1)}, bf16[128,2048]{1,0:T(8,128)(2,1)}, u32[]{:S(2)}) copy-start(bf16[128,2048]{1,0:T(8,128)(2,1)} %param.31) | copy-start | bytes 1572868
  7.2 47.1 %copy-start.7 = (bf16[256,88]{0,1:T(8,128)(2,1)S(1)}, bf16[256,88]{0,1:T(8,128)(2,1)}, u32[]{:S(2)}) copy-start(bf16[256,88]{0,1:T(8,128)(2,1)} %param.20) | copy-start | bytes 135172
  7.2 120.8 %all-gather.3.cloned.1.call-start = ((), (), s32[]{:S(2)}) async-start(), calls=%async_computation.12 | async-start | bytes 2928640 | tf_op jit(solution)/shard_map/all_gather | solution.py:57
  9.4 34.3 %all-to-all-start = ((bf16[64,16,256]{2,1,0:T(8,128)(2,1)}), bf16[64,16,256]{2,1,0:T(8,128)(2,1)S(1)}, u32[]{:S(2)}, u32[]{:S(2)}) async-start(bf16[64,16,256]{2,1,0:T(8,128)(2,1)} %broadcast_in_dim.18), calls=%async_computation | async-start | bytes 1048576 | tf_op jit(solution)/shard_map/all_to_all | solution.py:11
  46.0 12.9 %all-to-all-start.2 = ((bf16[8,2,512]{2,1,0:T(2,128)(2,1)}), bf16[8,2,512]{2,1,0:T(2,128)(2,1)S(1)}, u32[]{:S(2)}, u32[]{:S(2)}) async-start(bf16[8,2,512]{2,1,0:T(2,128)(2,1)} %reshape.192), calls=%async_computation.2 | async-start | bytes 32768 | tf_op jit(solution)/shard_map/all_to_all | solution.py:11
  54.3 10.0 %copy-start.8 = (bf16[256,88]{0,1:T(8,128)(2,1)S(1)}, bf16[256,88]{0,1:T(8,128)(2,1)}, u32[]{:S(2)}) copy-start(bf16[256,88]{0,1:T(8,128)(2,1)} %param.21) | copy-start | bytes 135172
  60.2 23.3 %all-to-all-start.1 = ((bf16[8,1024,88]{1,2,0:T(8,128)(2,1)}), bf16[8,1024,88]{1,2,0:T(8,128)(2,1)S(1)}, u32[]{:S(2)}, u32[]{:S(2)}) async-start(bf16[8,1024,88]{1,2,0:T(8,128)(2,1)} %broadcast_in_dim.19), calls=%async_computation.1 | async-start | bytes 2883584 | tf_op jit(solution)/shard_map/all_to_all | solution.py:11
  84.8 23.7 %all-to-all-start.3 = ((bf16[8,1024,88]{1,2,0:T(8,128)(2,1)}), bf16[8,1024,88]{1,2,0:T(8,128)(2,1)S(1)}, u32[]{:S(2)}, u32[]{:S(2)}) async-start(bf16[8,1024,88]{1,2,0:T(8,128)(2,1)} %broadcast_in_dim.41), calls=%async_computation.3 | async-start | bytes 2883584 | tf_op jit(solution)/shard_map/all_to_all | solution.py:11
  91.6 36.4 %copy-start.11 = (bf16[16,256]{1,0:T(8,128)(2,1)S(1)}, bf16[16,256]{1,0:T(8,128)(2,1)}, u32[]{:S(2)}) copy-start(bf16[16,256]{1,0:T(8,128)(2,1)} %param.18) | copy-start | bytes 24580
  108.9 28.5 %copy-start.13 = (f32[128]{0:T(128)S(1)}, f32[128]{0:T(128)}, u32[]{:S(2)}) copy-start(f32[128]{0:T(128)} %param.28) | copy-start | bytes 1540
  108.9 28.5 %copy-start.12 = (bf16[2048]{0:T(1024)(128)(2,1)S(1)}, bf16[2048]{0:T(1024)(128)(2,1)}, u32[]{:S(2)}) copy-start(bf16[2048]{0:T(1024)(128)(2,1)} %param.23) | copy-start | bytes 12292
  108.9 28.5 %copy-start.14 = (bf16[128]{0:T(256)(128)(2,1)S(1)}, bf16[128]{0:T(256)(128)(2,1)}, u32[]{:S(2)}) copy-start(bf16[128]{0:T(256)(128)(2,1)} %param.30) | copy-start | bytes 772
  109.9 32.7 %copy-start.3 = (bf16[2048,128]{1,0:T(8,128)(2,1)S(1)}, bf16[2048,128]{1,0:T(8,128)(2,1)}, u32[]{:S(2)}) copy-start(bf16[2048,128]{1,0:T(8,128)(2,1)} %param.26) | copy-start | bytes 1572868
  109.9 17.6 %all-to-all-start.4 = ((bf16[64,16,88]{2,1,0:T(8,128)(2,1)}), bf16[64,16,88]{2,1,0:T(8,128)(2,1)S(1)}, u32[]{:S(2)}, u32[]{:S(2)}) async-start(bf16[64,16,88]{2,1,0:T(8,128)(2,1)} %multiply_convert_fusion.1), calls=%async_computation.4 | async-start | bytes 524288 | tf_op jit(solution)/shard_map/all_to_all | solution.py:54
  114.8 28.0 %copy-start.4 = (bf16[2048,128]{1,0:T(8,128)(2,1)S(1)}, bf16[2048,128]{1,0:T(8,128)(2,1)}, u32[]{:S(2)}) copy-start(bf16[2048,128]{1,0:T(8,128)(2,1)} %param.24) | copy-start | bytes 1572868
  114.8 143.4 %all-gather.5.cloned.1.call-start = ((), (), s32[]{:S(2)}) async-start(), calls=%async_computation.13 | async-start | bytes 2928640 | tf_op jit(solution)/shard_map/all_gather | solution.py:57
  127.6 15.4 %copy-start.5 = (bf16[2048,128]{1,0:T(8,128)(2,1)S(1)}, bf16[2048,128]{1,0:T(8,128)(2,1)}, u32[]{:S(2)}) copy-start(bf16[2048,128]{1,0:T(8,128)(2,1)} %param.25) | copy-start | bytes 1572868
  127.9 15.3 %copy-start.2 = (f32[16,1,128,128]{3,2,1,0:T(8,128)S(1)}, f32[16,1,128,128]{3,2,1,0:T(8,128)}, u32[]{:S(2)}) copy-start(f32[16,1,128,128]{3,2,1,0:T(8,128)} %param.29) | copy-start | bytes 3145732
  131.0 11.3 %all-to-all-start.5 = ((bf16[8,16,256]{2,1,0:T(8,128)(2,1)}), bf16[8,16,256]{2,1,0:T(8,128)(2,1)S(1)}, u32[]{:S(2)}, u32[]{:S(2)}) async-start(bf16[8,16,256]{2,1,0:T(8,128)(2,1)} %broadcast_in_dim.42), calls=%async_computation.5 | async-start | bytes 131072 | tf_op jit(solution)/shard_map/all_to_all | solution.py:11
  142.8 3.2 %copy-start.6 = (bf16[2048,128]{1,0:T(8,128)(2,1)S(1)}, bf16[2048,128]{1,0:T(8,128)(2,1)}, u32[]{:S(2)}) copy-start(bf16[2048,128]{1,0:T(8,128)(2,1)} %param.27) | copy-start | bytes 1572868
  143.2 16.6 %copy-start.15 = (bf16[256]{0:T(256)(128)(2,1)S(1)}, bf16[256]{0:T(256)(128)(2,1)}, u32[]{:S(2)}) copy-start(bf16[256]{0:T(256)(128)(2,1)} %param.32) | copy-start | bytes 1540
  143.9 1.0 copy-start.1
  144.8 40.7 %copy-start.9 = (bf16[256,88]{0,1:T(8,128)(2,1)S(1)}, bf16[256,88]{0,1:T(8,128)(2,1)}, u32[]{:S(2)}) copy-start(bf16[256,88]{0,1:T(8,128)(2,1)} %param.33) | copy-start | bytes 135172
  155.2 22.2 %all-to-all-start.7 = ((bf16[64,16,256]{2,1,0:T(8,128)(2,1)}), bf16[64,16,256]{2,1,0:T(8,128)(2,1)S(1)}, u32[]{:S(2)}, u32[]{:S(2)}) async-start(bf16[64,16,256]{2,1,0:T(8,128)(2,1)} %broadcast_in_dim.43), calls=%async_computation.7 | async-start | bytes 1048576 | tf_op jit(solution)/shard_map/all_to_all | solution.py:11
  179.1 11.0 %all-to-all-start.9 = ((bf16[8,2,512]{2,1,0:T(2,128)(2,1)}), bf16[8,2,512]{2,1,0:T(2,128)(2,1)S(1)}, u32[]{:S(2)}, u32[]{:S(2)}) async-start(bf16[8,2,512]{2,1,0:T(2,128)(2,1)} %reshape.194), calls=%async_computation.9 | async-start | bytes 32768 | tf_op jit(solution)/shard_map/all_to_all | solution.py:11
  185.5 10.0 %copy-start.10 = (bf16[256,88]{0,1:T(8,128)(2,1)S(1)}, bf16[256,88]{0,1:T(8,128)(2,1)}, u32[]{:S(2)}) copy-start(bf16[256,88]{0,1:T(8,128)(2,1)} %param.34) | copy-start | bytes 135172
  191.4 23.4 %all-to-all-start.8 = ((bf16[8,1024,88]{1,2,0:T(8,128)(2,1)}), bf16[8,1024,88]{1,2,0:T(8,128)(2,1)S(1)}, u32[]{:S(2)}, u32[]{:S(2)}) async-start(bf16[8,1024,88]{1,2,0:T(8,128)(2,1)} %broadcast_in_dim.44), calls=%async_computation.8 | async-start | bytes 2883584 | tf_op jit(solution)/shard_map/all_to_all | solution.py:11
  216.1 23.7 %all-to-all-start.10 = ((bf16[8,1024,88]{1,2,0:T(8,128)(2,1)}), bf16[8,1024,88]{1,2,0:T(8,128)(2,1)S(1)}, u32[]{:S(2)}, u32[]{:S(2)}) async-start(bf16[8,1024,88]{1,2,0:T(8,128)(2,1)} %broadcast_in_dim.46), calls=%async_computation.10 | async-start | bytes 2883584 | tf_op jit(solution)/shard_map/all_to_all | solution.py:11
Sparse Core Ops, SparseCore 0:
  11.0 87.9 all-gather.2
  118.7 80.6 all-gather.4
where the time goes:
time: 270 us; the launch traced here: 268 us
  waiting for transfers between devices  132 us (49%)
  starting transfers between devices  64.8 us (24%)
  blocking collectives  25.4 us (9%)
  local copies, waits for them, and re-layouts  15 us (6%)
  between operations  14.5 us (5%)
  matrix products  8.37 us (3%)
  other arithmetic  7.49 us (3%)
    all_to_all x9, waiting for transfers between devices, sent_to_all(): return lax.all_to_all(copies, axis, split_axis=0, concat_axis=0, tiled=True)  119 us
    all_to_all x9, starting transfers between devices, sent_to_all(): return lax.all_to_all(copies, axis, split_axis=0, concat_axis=0, tiled=True)  59.8 us
    all_to_all x1, blocking collectives, feed_forward(): lax.all_to_all(inner_units, 'kv', split_axis=0, concat_axis=1, tiled=True)  17.3 us
    all_to_all x1, waiting for transfers between devices, feed_forward(): lax.all_to_all(inner_units, 'kv', split_axis=0, concat_axis=1, tiled=True)  11.9 us
    broadcast_in_dim x10, local copies, waits for them, and re-layouts, sent_to_all(): copies = jnp.broadcast_to(shard, (lax.axis_size(axis), *shard.shape))  8.75 us
    all_to_all x1, blocking collectives, sum_at_owner(): blocks = lax.all_to_all(split_up(shard, dim, count), axis, 0, 0, tiled=True)  8.05 us
  transfers between devices with their start and end apart: 12, of which 10 were waited for; matrix products, arithmetic and copies ran while one was open for 10% of the time, Pallas kernels for 0%

commit v1 on v0

v1 whole, which is shorter than its diff:
```python
import functools

import jax
import jax.numpy as jnp
from jax import lax
from jax.experimental import pallas as pl
from jax.experimental.pallas import tpu as pltpu
from jax.sharding import PartitionSpec as P

MESH = pl.DeviceIdType.MESH
F32 = jnp.float32
BF16 = jnp.bfloat16
ROWS = 16
WIDTH = 256
HALF = 128
HID = 88
HEAD = 128
GATE, UP, DOWN = 0, 1, 2
ROW_DIMS = (((1,), (1,)), ((), ()))


def kernel(
    n,
    hidden_hbm,
    params_hbm,
    gate1_hbm,
    up1_hbm,
    down1_hbm,
    gate2_hbm,
    up2_hbm,
    down2_hbm,
    query_hbm,
    forget_hbm,
    input_hbm,
    outgate_hbm,
    mixout_hbm,
    state_hbm,
    hidden_out_hbm,
    state_out_hbm,
    hid,
    par,
    gains,
    weights,
    wmix,
    wout,
    state,
    act,
    part,
    red0,
    red1,
    sum0,
    sum1,
    own0,
    own1,
    mid,
    rows_in,
    mix_send,
    mix_recv,
    last,
    load_sem,
    gain_send,
    gain_recv,
    w_send,
    w_recv,
    a_send,
    a_recv,
    b_send,
    b_recv,
    c_send,
    c_recv,
    d_send,
    d_recv,
    x_send,
    x_recv,
    m_send,
    m_recv,
):
    kv = lax.axis_index("kv")
    tp = lax.axis_index("tp")
    z, y = lax.div(kv, n), lax.rem(kv, n)
    group = lax.rem(z + y, n)
    src_y = lax.rem(tp - z + n, n)
    src_z = lax.rem(tp - y + n, n)
    home = tp == group
    pair = tp + 1 - 2 * lax.rem(tp, 2)
    far_first = sorted(range(1, n), key=lambda d: -min(d, n - d))

    def at(zz, yy, tt):
        return {"kv": zz * n + yy, "tp": tt}

    def up(index, d):
        return lax.rem(index + d, n)

    def rows_of(zz):
        return pl.ds(pl.multiple_of(zz * ROWS, ROWS), ROWS)

    loads = [
        pltpu.make_async_copy(hidden_hbm, hid, load_sem.at[0]),
        pltpu.make_async_copy(params_hbm, par, load_sem.at[1]),
        pltpu.make_async_copy(gate1_hbm, weights.at[0, tp, GATE], load_sem.at[2]),
        pltpu.make_async_copy(up1_hbm, weights.at[0, tp, UP], load_sem.at[3]),
        pltpu.make_async_copy(down1_hbm, weights.at[0, tp, DOWN], load_sem.at[4]),
        pltpu.make_async_copy(gate2_hbm, weights.at[1, tp, GATE], load_sem.at[5]),
        pltpu.make_async_copy(up2_hbm, weights.at[1, tp, UP], load_sem.at[6]),
        pltpu.make_async_copy(down2_hbm, weights.at[1, tp, DOWN], load_sem.at[7]),
        pltpu.make_async_copy(query_hbm, wmix.at[:, 0:HEAD], load_sem.at[8]),
        pltpu.make_async_copy(forget_hbm, wmix.at[:, HEAD : 2 * HEAD], load_sem.at[9]),
        pltpu.make_async_copy(input_hbm, wmix.at[:, 2 * HEAD : 3 * HEAD], load_sem.at[10]),
        pltpu.make_async_copy(outgate_hbm, wmix.at[:, 3 * HEAD :], load_sem.at[11]),
        pltpu.make_async_copy(mixout_hbm, wout, load_sem.at[12]),
        pltpu.make_async_copy(state_hbm, state, load_sem.at[13]),
    ]
    for load in loads:
        load.start()

    barrier = pltpu.get_barrier_semaphore()

    def greet(device):
        pl.semaphore_signal(barrier, inc=1, device_id=device, device_id_type=MESH)

    for d in range(1, n):
        greet(at(z, y, up(tp, d)))
        greet(at(up(z, d), y, tp))
        greet(at(z, up(y, d), tp))
        greet(at(z, up(y, d), group))
        greet(at(up(z, d), y, group))

    @pl.when(jnp.logical_not(home))
    def _():
        for d in range(n):
            greet(at(z, src_y, up(tp, d)))
            greet(at(src_z, y, up(tp, d)))

    for load in loads[:8]:
        load.wait()
    gains[tp] = par[8:16]

    pl.semaphore_wait(barrier, 5 * (n - 1) + jnp.where(home, 0, 2 * n))

    sends = []

    def send(src, dst, send_sem, recv_sem, device):
        copy = pltpu.make_async_remote_copy(
            src_ref=src,
            dst_ref=dst,
            send_sem=send_sem,
            recv_sem=recv_sem,
            device_id=device,
            device_id_type=MESH,
        )
        copy.start()
        sends.append((copy, None))

    def send_or_keep(here, src, dst, send_sem, recv_sem, device):
        away = pltpu.make_async_remote_copy(
            src_ref=src,
            dst_ref=dst,
            send_sem=send_sem,
            recv_sem=recv_sem,
            device_id=device,
            device_id_type=MESH,
        )

        @pl.when(here)
        def _():
            pltpu.make_async_copy(src, dst, recv_sem).start()

        @pl.when(jnp.logical_not(here))
        def _():
            away.start()

        sends.append((away, here))

    def arrived(dst, sem):
        pltpu.make_async_copy(dst, dst, sem).wait()

    def weights_of(kind, f, slot):
        return weights.at[f, slot, GATE:DOWN] if kind == 0 else weights.at[f, slot, DOWN]

    def send_weights(kind, f):
        for k in range(1, n // 2):
            send(
                weights_of(kind, f, tp),
                weights_of(kind, f, tp),
                w_send.at[kind, f, k],
                w_recv.at[kind, f, tp],
                at(z, y, up(tp, 2 * k)),
            )
        send(weights_of(kind, f, tp), weights_of(kind, f, tp), w_send.at[kind, f, 0], w_recv.at[kind, f, tp], at(z, y, pair))

    def pass_weights(kind, f):
        for k in range(1, n // 2):
            slot = up(tp, 2 * k)
            arrived(weights_of(kind, f, slot), w_recv.at[kind, f, slot])
            send(
                weights_of(kind, f, slot),
                weights_of(kind, f, slot),
                w_send.at[kind, f, n // 2 + k],
                w_recv.at[kind, f, slot],
                at(z, y, pair),
            )

    def take_weights(kind, f):
        for k in range(n // 2):
            slot = up(pair, 2 * k)
            arrived(weights_of(kind, f, slot), w_recv.at[kind, f, slot])

    def spread(f, block):
        for d in [0] + far_first:
            to_row = at(z, up(y, d), group)
            to_col = at(up(z, d), y, group)
            row_args = (
                block.at[:, 0:HALF],
                act.at[f, tp, rows_of(z), 0:HALF],
                a_send.at[f, 0, d],
                a_recv.at[f, 0, tp],
                to_row,
            )
            col_args = (
                block.at[:, HALF:WIDTH],
                act.at[f, tp, rows_of(z), HALF:WIDTH],
                a_send.at[f, 1, d],
                a_recv.at[f, 1, tp],
                to_col,
            )
            if d == 0:
                send_or_keep(home, *row_args)
                send_or_keep(home, *col_args)
            else:
                send(*row_args)
                send(*col_args)

    def gather(f):
        for t in range(n):
            arrived(act.at[f, t, rows_of(z), 0:HALF], a_recv.at[f, 0, t])
        region = act.at[f, :, rows_of(z), 0:HALF]
        for d in far_first:
            send(region, region, b_send.at[f, 0, d], b_recv.at[f, 0, d], at(up(z, d), y, tp))
        for t in range(n):
            arrived(act.at[f, t, rows_of(src_z), HALF:WIDTH], a_recv.at[f, 1, t])
        region = act.at[f, :, rows_of(src_z), HALF:WIDTH]
        for d in far_first:
            send(region, region, b_send.at[f, 1, d], b_recv.at[f, 1, d], at(z, up(y, d), tp))

    def gathered(f):
        for d in range(1, n):
            arrived(act.at[f, :, rows_of(up(z, n - d)), 0:HALF], b_recv.at[f, 0, d])
            arrived(
                act.at[f, :, rows_of(up(src_z, d)), HALF:WIDTH], b_recv.at[f, 1, d]
            )

    def inner_units(f):
        gate = jnp.zeros((n * ROWS, HID), F32)
        up_total = jnp.zeros((n * ROWS, HID), F32)
        squares = jnp.zeros((n * ROWS, HALF), F32)
        for t in range(n):
            values = act[f, t].astype(F32)
            squares += values[:, 0:HALF] * values[:, 0:HALF]
            squares += values[:, HALF:WIDTH] * values[:, HALF:WIDTH]
            scaled = (values * gains[t, f : f + 1, :]).astype(BF16)
            gate += lax.dot_general(scaled, weights[f, t, GATE], ROW_DIMS, preferred_element_type=F32)
            up_total += lax.dot_general(scaled, weights[f, t, UP], ROW_DIMS, preferred_element_type=F32)
        inverse = lax.rsqrt(jnp.sum(squares, axis=1, keepdims=True) / (n * WIDTH) + 1e-06)
        gate = gate * inverse
        return (gate * jax.nn.sigmoid(gate) * (up_total * inverse)).astype(BF16)

    def scatter(f, units):
        for t in range(n):
            part[f, t] = jnp.dot(
                units, weights[f, t, DOWN], preferred_element_type=F32
            ).astype(BF16)
        for d in far_first:
            to_z, to_y = up(z, d), up(y, d)
            send(
                part.at[f, :, rows_of(to_z), 0:HALF],
                red0.at[f, d],
                c_send.at[f, 0, d],
                c_recv.at[f, 0, d],
                at(to_z, y, tp),
            )
            send(
                part.at[f, :, rows_of(lax.rem(tp - to_y + n, n)), HALF:WIDTH],
                red1.at[f, d],
                c_send.at[f, 1, d],
                c_recv.at[f, 1, d],
                at(z, to_y, tp),
            )

    def reduce(f):
        for half, red, summed, lanes, row in (
            (0, red0, sum0, slice(0, HALF), z),
            (1, red1, sum1, slice(HALF, WIDTH), src_z),
        ):
            total = part[f, :, rows_of(row), lanes].astype(F32)
            for d in range(1, n):
                arrived(red.at[f, d], c_recv.at[f, half, d])
                total += red[f, d].astype(F32)
            summed[f] = total.astype(BF16)
            for e in [0] + far_first:
                tt = up(tp, e)
                if half == 0:
                    args = (sum0.at[f, tt], own0.at[f, y], d_send.at[f, 0, e], d_recv.at[f, 0, y])
                    device = at(z, src_y, tt)
                else:
                    args = (sum1.at[f, tt], own1.at[f, z], d_send.at[f, 1, e], d_recv.at[f, 1, z])
                    device = at(src_z, y, tt)
                if e == 0:
                    send_or_keep(home, *args, device)
                else:
                    send(*args, device)

    def reduced(f):
        for k in range(n):
            arrived(own0.at[f, k], d_recv.at[f, 0, k])
            arrived(own1.at[f, k], d_recv.at[f, 1, k])
        left = jnp.sum(own0[f].astype(F32), axis=0)
        right = jnp.sum(own1[f].astype(F32), axis=0)
        return jnp.concatenate([left, right], axis=1)

    for d in range(1, n):
        send(gains.at[tp], gains.at[tp], gain_send.at[d], gain_recv.at[d], at(z, y, up(tp, d)))
    spread(0, hid)
    send_weights(0, 0)
    send_weights(1, 0)
    gather(0)
    pass_weights(0, 0)
    pass_weights(1, 0)
    for d in range(1, n):
        arrived(gains.at[up(tp, n - d)], gain_recv.at[d])
    take_weights(0, 0)
    gathered(0)
    units = inner_units(0)
    take_weights(1, 0)
    scatter(0, units)
    send_weights(0, 1)
    send_weights(1, 1)
    reduce(0)
    pass_weights(0, 1)
    pass_weights(1, 1)
    first = (hid[...].astype(F32) + 0.5 * reduced(0)).astype(BF16)

    rows_in[tp] = first
    for d in range(1, n):
        send(rows_in.at[tp], rows_in.at[tp], x_send.at[d], x_recv.at[d], at(z, y, up(tp, d)))
    for load in loads[8:]:
        load.wait()
    for d in range(1, n):
        arrived(rows_in.at[up(tp, n - d)], x_recv.at[d])
    squares = jnp.zeros((ROWS, WIDTH), F32)
    for t in range(n):
        values = rows_in[t].astype(F32)
        squares += values * values
    inverse = lax.rsqrt(jnp.sum(squares, axis=1, keepdims=True) / (n * WIDTH) + 1e-06)
    projected = jnp.zeros((ROWS, 4 * HEAD), F32)
    for t in range(n):
        normed = (rows_in[t].astype(F32) * inverse * par[t : t + 1, :]).astype(BF16)
        projected += jnp.dot(
            normed, wmix[t * WIDTH : (t + 1) * WIDTH, :], preferred_element_type=F32
        )
    query = projected[:, 0:HEAD]
    query = query * jax.nn.sigmoid(query)
    floor = par[10:11, 0:HEAD]
    keep = floor + (1.0 - floor) * jax.nn.sigmoid(projected[:, HEAD : 2 * HEAD])
    fresh = (1.0 - floor) * jax.nn.sigmoid(-projected[:, HEAD : 2 * HEAD])
    value = projected[:, 2 * HEAD : 3 * HEAD]
    outgate = projected[:, 3 * HEAD :]
    columns = jnp.concatenate(
        [keep, fresh, query, jnp.zeros((HEAD - 3 * ROWS, HEAD), F32)], axis=0
    ).T
    readout = []
    for b in range(ROWS):
        updated = (
            columns[:, b : b + 1] * state[b]
            + columns[:, ROWS + b : ROWS + b + 1] * value[b : b + 1, :]
        )
        state[b] = updated
        readout.append(
            jnp.sum(columns[:, 2 * ROWS + b : 2 * ROWS + b + 1] * updated, axis=0, keepdims=True)
        )
    readout = jnp.concatenate(readout, axis=0)
    normed = (
        readout
        * lax.rsqrt(jnp.mean(readout * readout, axis=1, keepdims=True) + 1e-05)
        * par[10:11, HEAD : 2 * HEAD]
    )
    gated = (normed * (outgate * jax.nn.sigmoid(outgate))).astype(BF16)
    for t in range(n):
        mix_send[t] = jnp.dot(
            gated, wout[:, t * WIDTH : (t + 1) * WIDTH], preferred_element_type=F32
        ).astype(BF16)
    for d in range(1, n):
        to = up(tp, d)
        send(mix_send.at[to], mix_recv.at[d], m_send.at[d], m_recv.at[d], at(z, y, to))
    store_state = pltpu.make_async_copy(state, state_out_hbm, load_sem.at[14])
    store_state.start()
    mixed = mix_send[tp].astype(F32)
    for d in range(1, n):
        arrived(mix_recv.at[d], m_recv.at[d])
        mixed += mix_recv[d].astype(F32)
    second = (first.astype(F32) + mixed).astype(BF16)
    mid[...] = second

    spread(1, mid)
    gather(1)
    take_weights(0, 1)
    take_weights(1, 1)
    gathered(1)
    scatter(1, inner_units(1))
    reduce(1)
    last[...] = (second.astype(F32) + 0.5 * reduced(1)).astype(BF16)
    store = pltpu.make_async_copy(last, hidden_out_hbm, load_sem.at[15])
    store.start()
    for copy, here in sends:
        if here is None:
            copy.wait_send()
        else:

            @pl.when(jnp.logical_not(here))
            def _():
                copy.wait_send()

    store_state.wait()
    store.wait()


def layer(
    hidden_in,
    first_gain,
    first_gate_proj,
    first_up_proj,
    first_down_proj,
    mix_gain,
    query_weight,
    forget_weight,
    input_weight,
    outgate_weight,
    forget_floor,
    state_in,
    out_gain,
    mix_out_weight,
    second_gain,
    second_gate_proj,
    second_up_proj,
    second_down_proj,
):
    n = lax.axis_size("tp")
    assert lax.axis_size("kv") == n * n
    params = jnp.concatenate(
        [
            jnp.pad(mix_gain.astype(F32).reshape(n, WIDTH), ((0, 8 - n), (0, 0))),
            first_gain.astype(F32)[None],
            second_gain.astype(F32)[None],
            jnp.concatenate([forget_floor, out_gain.astype(F32)])[None],
            jnp.zeros((5, WIDTH), F32),
        ]
    )
    state_shape = (ROWS, HEAD, HEAD)
    dma = pltpu.SemaphoreType.DMA
    vmem = pltpu.VMEM
    any_space = pl.BlockSpec(memory_space=pl.ANY)
    hidden_out, state_out = pl.pallas_call(
        functools.partial(kernel, n),
        out_shape=(
            jax.ShapeDtypeStruct((ROWS, WIDTH), BF16),
            jax.ShapeDtypeStruct(state_shape, F32),
        ),
        in_specs=[any_space] * 14,
        out_specs=(any_space, any_space),
        scratch_shapes=[
            vmem((ROWS, WIDTH), BF16),
            vmem((16, WIDTH), F32),
            vmem((n, 8, WIDTH), F32),
            vmem((2, n, 3, HID, WIDTH), BF16),
            vmem((n * WIDTH, 4 * HEAD), BF16),
            vmem((HEAD, n * WIDTH), BF16),
            vmem(state_shape, F32),
            vmem((2, n, n * ROWS, WIDTH), BF16),
            vmem((2, n, n * ROWS, WIDTH), BF16),
            vmem((2, n, n, ROWS, HALF), BF16),
            vmem((2, n, n, ROWS, HALF), BF16),
            vmem((2, n, ROWS, HALF), BF16),
            vmem((2, n, ROWS, HALF), BF16),
            vmem((2, n, ROWS, HALF), BF16),
            vmem((2, n, ROWS, HALF), BF16),
            vmem((ROWS, WIDTH), BF16),
            vmem((n, ROWS, WIDTH), BF16),
            vmem((n, ROWS, WIDTH), BF16),
            vmem((n, ROWS, WIDTH), BF16),
            vmem((ROWS, WIDTH), BF16),
            dma((16,)),
            dma((n,)),
            dma((n,)),
            dma((2, 2, n)),
            dma((2, 2, n)),
            dma((2, 2, n)),
            dma((2, 2, n)),
            dma((2, 2, n)),
            dma((2, 2, n)),
            dma((2, 2, n)),
            dma((2, 2, n)),
            dma((2, 2, n)),
            dma((2, 2, n)),
            dma((n,)),
            dma((n,)),
            dma((n,)),
            dma((n,)),
        ],
        compiler_params=pltpu.CompilerParams(
            collective_id=0, has_side_effects=True, vmem_limit_bytes=60 * 1024 * 1024
        ),
        name="layer",
    )(
        hidden_in,
        params,
        first_gate_proj.T,
        first_up_proj.T,
        first_down_proj,
        second_gate_proj.T,
        second_up_proj.T,
        second_down_proj,
        query_weight,
        forget_weight,
        input_weight,
        outgate_weight,
        mix_out_weight,
        state_in.reshape(state_shape),
    )
    return hidden_out, state_out.reshape(ROWS, 1, HEAD, HEAD)


def solution(mesh):
    placed = (
        P("kv", "tp"),
        P("tp"),
        P("tp", "kv"),
        P("tp", "kv"),
        P("kv", "tp"),
        P(),
        P(None, "tp"),
        P(None, "tp"),
        P(None, "tp"),
        P(None, "tp"),
        P("tp"),
        P("kv", "tp", None, None),
        P("tp"),
        P("tp", None),
        P("tp"),
        P("tp", "kv"),
        P("tp", "kv"),
        P("kv", "tp"),
    )
    return jax.shard_map(
        layer,
        mesh=mesh,
        in_specs=placed,
        out_specs=(P("kv", "tp"), P("kv", "tp", None, None)),
        check_vma=False,
    )
```

time: 270 us -> 90.7 us (0.34)
  waiting for transfers between devices: 132 us -> 0 us
  Pallas kernels: 0 us -> 82 us
  starting transfers between devices: 64.8 us -> 0 us
  blocking collectives: 25.4 us -> 0 us
  between operations: 14.5 us -> 0.67 us
  matrix products: 8.37 us -> 0 us
  local copies, waits for them, and re-layouts: 15 us -> 7.44 us
  other arithmetic: 7.49 us -> 0.01 us
    all_to_all x10 -> x0, waiting for transfers between devices: 131 us -> none  [the longest x9 119 us: sent_to_all(): return lax.all_to_all(copies, axis, split_axis=0, concat_axis=0, tiled=True)]
    pallas_call x0 -> x1, Pallas kernels: none -> 82 us  [layer(): pl.pallas_call(functools.partial(kernel, n), out_shape=(jax.ShapeDtypeStr...]
    all_to_all x10 -> x0, starting transfers between devices: 64.8 us -> none  [the longest x9 59.8 us: sent_to_all(): return lax.all_to_all(copies, axis, split_axis=0, concat_axis=0, tiled=True)]
    all_to_all x2 -> x0, blocking collectives: 25.4 us -> none  [the longest x1 17.3 us: feed_forward(): lax.all_to_all(inner_units, 'kv', split_axis=0, concat_axis=1, tiled=True)]
    broadcast_in_dim x10 -> x1, local copies, waits for them, and re-layouts: 8.75 us -> 0.01 us  [layer(): jnp.zeros((5, WIDTH), F32)]
    dot_general x11 -> x0, matrix products: 8.37 us -> none  [the longest x2 5.28 us: feed_forward(): jnp.dot(own_units, lax.all_gather(down_proj, 'kv', axis=0, tiled=True), p...]
    unnamed x36 -> x12, local copies, waits for them, and re-layouts: 2.32 us -> 6.22 us
    reduce_sum x11 -> x0, other arithmetic: 3.23 us -> none  [the longest x6 2.51 us: taken_together(): return sent_to_all(shard, axis).astype(jnp.float32).sum(axis=0)]
  transfers between devices with their start and end apart: 12 -> 0, of which waited for: 10 -> 0; matrix products, arithmetic and copies ran while one was open for 10% -> 0% of each run, Pallas kernels for 0% -> 0%
where the time goes in v1:
time: 90.7 us; the launch traced here: 90.1 us
  Pallas kernels  82 us (90%)
  local copies, waits for them, and re-layouts  7.44 us (8%)
    pallas_call x1, Pallas kernels, layer(): pl.pallas_call(functools.partial(kernel, n), out_shape=(jax.ShapeDtypeStr...  82 us
    unnamed x12, local copies, waits for them, and re-layouts  6.22 us

profile of v1, /device:TPU:1, one launch (start us, length us, event | category | flops | bytes accessed | tf_op | source)
XLA Modules:
  0.0 90.1 jit_solution(9202023226118729133)
XLA Ops:
  0.6 0.0 copy-start.2
  0.6 0.6 copy-done.2
  1.3 0.0 copy-start.1
  1.3 0.7 copy-done.1
  1.9 0.0 copy-start.3
  2.0 0.0 copy-start.4
  2.0 0.6 copy-done.3
  2.6 0.0 copy-start
  2.6 0.0 copy-done.4
  2.6 0.7 copy-done
  3.3 1.2 %concatenate.7.params_hbm = f32[16,256]{1,0:T(8,128)} concatenate(f32[8,256]{1,0:T(8,128)S(1)} %reshape.21, f32[1,256]{1,0:T(1,128)S(1)} %bitcast.18, f32[1,256]{1,0:T(1,128)S(1)} %bitcast.19, f32[1,256]{1,0:T(1,128)S(1)} %bitcast.17, f32[5,256]{1,0:T(8,128)S(1)} %broadcast_in_dim.23), dimensions={0} | concatenate | bytes 32768 | tf_op jit(solution)/shard_map/concatenate | solution.py:448
  4.5 82.0 %layer.1 = (bf16[16,256]{1,0:T(8,128)(2,1)}, f32[16,128,128]{2,1,0:T(8,128)}) custom-call(bf16[16,256]{1,0:T(8,128)(2,1)} %hidden_hbm.1, f32[16,256]{1,0:T(8,128)} %concatenate.7.params_hbm, bf16[88,256]{1,0:T(8,128)(2,1)} %bitcast.13, bf16[88,256]{1,0:T(8,128)(2,1)} %bitcast.14, bf16[88,256]{1,0:T(8,128)(2,1)} %down1_hbm.1, bf16[88,256]{1,0:T(8,128)(2,1)} %bitcast.15, ...), custom_call_target="tpu_custom_call" | custom-call | tf_op jit(solution)/shard_map/layer/pallas_call | solution.py:461
  86.5 1.3 %copy.23 = bf16[16,256]{1,0:T(8,128)(2,1)} copy(bf16[16,256]{1,0:T(8,128)(2,1)} %get-tuple-element.10) | data formatting | bytes 16384
  87.8 2.3 %copy.24 = f32[16,1,128,128]{3,2,1,0:T(8,128)} copy(f32[16,1,128,128]{3,2,1,0:T(8,128)} %bitcast.11) | data formatting | bytes 2097152
  (6 shorter events, 0.0 us)
Async XLA Ops:
  0.6 0.7 copy-start.2
  1.3 0.7 copy-start.1
  1.9 0.7 copy-start.3
  2.0 0.7 copy-start.4
  2.6 0.7 copy-start

commit v2 on v1

v2 whole, which is shorter than its diff:
```python
import functools

import jax
import jax.numpy as jnp
from jax import lax
from jax.experimental import pallas as pl
from jax.experimental.pallas import tpu as pltpu
from jax.sharding import PartitionSpec as P

MESH = pl.DeviceIdType.MESH
F32 = jnp.float32
BF16 = jnp.bfloat16
ROWS = 16
WIDTH = 256
HALF = 128
HID = 88
HEAD = 128
PIECES = 4
GATE, UP, DOWN = 0, 1, 2
ROW_DIMS = (((1,), (1,)), ((), ()))


def kernel(
    n,
    hidden_hbm,
    mix_gain_hbm,
    first_gain_hbm,
    second_gain_hbm,
    floor_hbm,
    out_gain_hbm,
    gate1_hbm,
    up1_hbm,
    down1_hbm,
    gate2_hbm,
    up2_hbm,
    down2_hbm,
    query_hbm,
    forget_hbm,
    input_hbm,
    outgate_hbm,
    mixout_hbm,
    state_hbm,
    hidden_out_hbm,
    state_out_hbm,
    hid,
    mix_gain,
    own_gains,
    floor_in,
    out_gain,
    gains,
    weights,
    wmix,
    wout,
    state,
    act,
    part,
    red0,
    red1,
    sum0,
    sum1,
    own0,
    own1,
    mid,
    rows_in,
    mix_send,
    mix_recv,
    last,
    load_sem,
    gain_send,
    gain_recv,
    w_send,
    w_recv,
    p_send,
    p_recv,
    a_send,
    a_recv,
    b_send,
    b_recv,
    c_send,
    c_recv,
    d_send,
    d_recv,
    x_send,
    x_recv,
    m_send,
    m_recv,
):
    kv = lax.axis_index("kv")
    tp = lax.axis_index("tp")
    z, y = lax.div(kv, n), lax.rem(kv, n)
    group = lax.rem(z + y, n)
    src_y = lax.rem(tp - z + n, n)
    src_z = lax.rem(tp - y + n, n)
    home = tp == group
    pair = tp + 1 - 2 * lax.rem(tp, 2)
    far_first = sorted(range(1, n), key=lambda d: -min(d, n - d))

    def at(zz, yy, tt):
        return {"kv": zz * n + yy, "tp": tt}

    def up(index, d):
        return lax.rem(index + d, n)

    def rows_of(zz):
        return pl.ds(pl.multiple_of(zz * ROWS, ROWS), ROWS)

    early = [
        (hidden_hbm, hid),
        (first_gain_hbm, own_gains.at[0]),
        (second_gain_hbm, own_gains.at[1]),
        (gate1_hbm, weights.at[0, tp, GATE]),
        (up1_hbm, weights.at[0, tp, UP]),
        (down1_hbm, weights.at[0, tp, DOWN]),
    ]
    later = [
        (gate2_hbm, weights.at[1, tp, GATE]),
        (up2_hbm, weights.at[1, tp, UP]),
        (down2_hbm, weights.at[1, tp, DOWN]),
        (mix_gain_hbm, mix_gain),
        (floor_hbm, floor_in),
        (out_gain_hbm, out_gain),
        (query_hbm, wmix.at[:, 0:HEAD]),
        (forget_hbm, wmix.at[:, HEAD : 2 * HEAD]),
        (input_hbm, wmix.at[:, 2 * HEAD : 3 * HEAD]),
        (outgate_hbm, wmix.at[:, 3 * HEAD :]),
        (mixout_hbm, wout),
        (state_hbm, state),
    ]
    loads = [
        pltpu.make_async_copy(src, dst, load_sem.at[i])
        for i, (src, dst) in enumerate(early + later)
    ]
    for load in loads:
        load.start()

    barrier = pltpu.get_barrier_semaphore()

    def greet(device):
        pl.semaphore_signal(barrier, inc=1, device_id=device, device_id_type=MESH)

    for d in range(1, n):
        greet(at(z, y, up(tp, d)))
        greet(at(up(z, d), y, tp))
        greet(at(z, up(y, d), tp))
        greet(at(z, up(y, d), group))
        greet(at(up(z, d), y, group))

    @pl.when(jnp.logical_not(home))
    def _():
        for d in range(n):
            greet(at(z, src_y, up(tp, d)))
            greet(at(src_z, y, up(tp, d)))

    with jax.named_scope("load"):
        for load in loads[: len(early)]:
            load.wait()
        for f in range(2):
            gains[tp, 2 * f : 2 * f + 2] = own_gains[f].astype(F32)

    with jax.named_scope("meet"):
        pl.semaphore_wait(barrier, 5 * (n - 1) + jnp.where(home, 0, 2 * n))

    def send(src, dst, send_sem, recv_sem, device):
        pltpu.make_async_remote_copy(
            src_ref=src,
            dst_ref=dst,
            send_sem=send_sem,
            recv_sem=recv_sem,
            device_id=device,
            device_id_type=MESH,
        ).start()

    def send_or_keep(here, src, dst, send_sem, recv_sem, device):
        @pl.when(here)
        def _():
            pltpu.make_async_copy(src, dst, recv_sem).start()

        @pl.when(jnp.logical_not(here))
        def _():
            send(src, dst, send_sem, recv_sem, device)

    def through(ref, sem):
        pltpu.make_async_copy(ref, ref, sem).wait()

    def weights_of(kind, f, slot):
        return weights.at[f, slot, GATE:DOWN] if kind == 0 else weights.at[f, slot, DOWN]

    def some_weights(kind, f, count):
        return weights.at[f, 0:count, GATE:DOWN] if kind == 0 else weights.at[f, 0:count, DOWN]

    def send_weights(kind, f):
        block = weights_of(kind, f, tp)
        for k in range(1, n // 2):
            send(block, block, w_send.at[kind, f], w_recv.at[kind, f], at(z, y, up(tp, 2 * k)))
        send(block, block, p_send.at[kind, f], p_recv.at[kind, f], at(z, y, pair))

    def pass_weights(kind, f):
        if n > 2:
            through(some_weights(kind, f, n // 2 - 1), w_recv.at[kind, f])
        for k in range(1, n // 2):
            block = weights_of(kind, f, up(tp, 2 * k))
            send(block, block, p_send.at[kind, f], p_recv.at[kind, f], at(z, y, pair))

    def take_weights(kind, f):
        through(some_weights(kind, f, n // 2), p_recv.at[kind, f])

    def weights_sent(kind, f):
        if n > 2:
            through(some_weights(kind, f, n // 2 - 1), w_send.at[kind, f])
        through(some_weights(kind, f, n // 2), p_send.at[kind, f])

    def spread(f, block):
        mine = act.at[f, tp, rows_of(z)]
        for d in [0] + far_first:
            for half, lanes, device in (
                (0, slice(0, HALF), at(z, up(y, d), group)),
                (1, slice(HALF, WIDTH), at(up(z, d), y, group)),
            ):
                args = (
                    block.at[:, lanes],
                    mine.at[:, lanes],
                    a_send.at[f, half],
                    a_recv.at[f, half],
                    device,
                )
                if d == 0:
                    send_or_keep(home, *args)
                else:
                    send(*args)

    def gather(f):
        for half, lanes, row in ((0, slice(0, HALF), z), (1, slice(HALF, WIDTH), src_z)):
            region = act.at[f, :, rows_of(row), lanes]
            through(region, a_recv.at[f, half])
            for d in far_first:
                device = at(up(z, d), y, tp) if half == 0 else at(z, up(y, d), tp)
                send(region, region, b_send.at[f, half], b_recv.at[f, half], device)

    def gathered(f):
        through(act.at[f, 0 : n - 1, :, 0:HALF], b_recv.at[f, 0])
        through(act.at[f, 0 : n - 1, :, HALF:WIDTH], b_recv.at[f, 1])

    def inner_units(f):
        gate = jnp.zeros((n * ROWS, HID), F32)
        up_total = jnp.zeros((n * ROWS, HID), F32)
        squares = jnp.zeros((n * ROWS, HALF), F32)
        for t in range(n):
            values = act[f, t].astype(F32)
            squares += values[:, 0:HALF] * values[:, 0:HALF]
            squares += values[:, HALF:WIDTH] * values[:, HALF:WIDTH]
            gain = jnp.concatenate(
                [gains[t, 2 * f : 2 * f + 1, :], gains[t, 2 * f + 1 : 2 * f + 2, :]], axis=1
            )
            scaled = (values * gain).astype(BF16)
            gate += lax.dot_general(scaled, weights[f, t, GATE], ROW_DIMS, preferred_element_type=F32)
            up_total += lax.dot_general(scaled, weights[f, t, UP], ROW_DIMS, preferred_element_type=F32)
        inverse = lax.rsqrt(jnp.sum(squares, axis=1, keepdims=True) / (n * WIDTH) + 1e-06)
        gate = gate * inverse
        return (gate * jax.nn.sigmoid(gate) * (up_total * inverse)).astype(BF16)

    def scatter(f, units):
        for t in range(n):
            part[f, t] = jnp.dot(
                units, weights[f, t, DOWN], preferred_element_type=F32
            ).astype(BF16)
        for d in far_first:
            to_z, to_y = up(z, d), up(y, d)
            send(
                part.at[f, :, rows_of(to_z), 0:HALF],
                red0.at[f, d],
                c_send.at[f, 0],
                c_recv.at[f, 0],
                at(to_z, y, tp),
            )
            send(
                part.at[f, :, rows_of(lax.rem(tp - to_y + n, n)), HALF:WIDTH],
                red1.at[f, d],
                c_send.at[f, 1],
                c_recv.at[f, 1],
                at(z, to_y, tp),
            )

    def reduce(f):
        for half, red, summed, lanes, row in (
            (0, red0, sum0, slice(0, HALF), z),
            (1, red1, sum1, slice(HALF, WIDTH), src_z),
        ):
            total = part[f, :, rows_of(row), lanes].astype(F32)
            through(red.at[f, 1:n], c_recv.at[f, half])
            for d in range(1, n):
                total += red[f, d].astype(F32)
            summed[f] = total.astype(BF16)
            for e in [0] + far_first:
                tt = up(tp, e)
                if half == 0:
                    args = (sum0.at[f, tt], own0.at[f, y], d_send.at[f, 0], d_recv.at[f, 0])
                    device = at(z, src_y, tt)
                else:
                    args = (sum1.at[f, tt], own1.at[f, z], d_send.at[f, 1], d_recv.at[f, 1])
                    device = at(src_z, y, tt)
                if e == 0:
                    send_or_keep(home, *args, device)
                else:
                    send(*args, device)

    def reduced(f):
        through(own0.at[f], d_recv.at[f, 0])
        through(own1.at[f], d_recv.at[f, 1])
        left = jnp.sum(own0[f].astype(F32), axis=0)
        right = jnp.sum(own1[f].astype(F32), axis=0)
        return jnp.concatenate([left, right], axis=1)

    with jax.named_scope("start"):
        for d in range(1, n):
            send(
                gains.at[tp], gains.at[tp], gain_send, gain_recv, at(z, y, up(tp, d))
            )
        spread(0, hid)
        send_weights(0, 0)
        send_weights(1, 0)
    with jax.named_scope("gather1"):
        gather(0)
    with jax.named_scope("pass1"):
        pass_weights(0, 0)
        pass_weights(1, 0)
        through(gains.at[1:n], gain_recv)
        take_weights(0, 0)
    with jax.named_scope("gathered1"):
        gathered(0)
    with jax.named_scope("inner1"):
        units = inner_units(0)
    with jax.named_scope("scatter1"):
        take_weights(1, 0)
        scatter(0, units)
        for load in loads[len(early) : len(early) + 3]:
            load.wait()
        send_weights(0, 1)
        send_weights(1, 1)
    with jax.named_scope("reduce1"):
        reduce(0)
    with jax.named_scope("pass2"):
        pass_weights(0, 1)
        pass_weights(1, 1)
    with jax.named_scope("reduced1"):
        first = (hid[...].astype(F32) + 0.5 * reduced(0)).astype(BF16)
        rows_in[tp] = first

    for d in range(1, n):
        send(rows_in.at[tp], rows_in.at[tp], x_send, x_recv, at(z, y, up(tp, d)))
    with jax.named_scope("rows"):
        for load in loads[len(early) + 3 :]:
            load.wait()
        through(rows_in.at[1:n], x_recv)
    squares = jnp.zeros((ROWS, WIDTH), F32)
    for t in range(n):
        values = rows_in[t].astype(F32)
        squares += values * values
    inverse = lax.rsqrt(jnp.sum(squares, axis=1, keepdims=True) / (n * WIDTH) + 1e-06)
    projected = jnp.zeros((ROWS, 4 * HEAD), F32)
    mix_gains = mix_gain[...].astype(F32)
    for t in range(n):
        gain = jnp.concatenate(
            [mix_gains[2 * t : 2 * t + 1, :], mix_gains[2 * t + 1 : 2 * t + 2, :]], axis=1
        )
        normed = (rows_in[t].astype(F32) * inverse * gain).astype(BF16)
        projected += jnp.dot(
            normed, wmix[t * WIDTH : (t + 1) * WIDTH, :], preferred_element_type=F32
        )
    query = projected[:, 0:HEAD]
    query = query * jax.nn.sigmoid(query)
    floor = floor_in[...]
    keep = floor + (1.0 - floor) * jax.nn.sigmoid(projected[:, HEAD : 2 * HEAD])
    fresh = (1.0 - floor) * jax.nn.sigmoid(-projected[:, HEAD : 2 * HEAD])
    value = projected[:, 2 * HEAD : 3 * HEAD]
    outgate = projected[:, 3 * HEAD :]
    columns = jnp.concatenate(
        [keep, fresh, query, jnp.zeros((HEAD - 3 * ROWS, HEAD), F32)], axis=0
    ).T
    readout = []
    for b in range(ROWS):
        updated = (
            columns[:, b : b + 1] * state[b]
            + columns[:, ROWS + b : ROWS + b + 1] * value[b : b + 1, :]
        )
        state[b] = updated
        readout.append(
            jnp.sum(columns[:, 2 * ROWS + b : 2 * ROWS + b + 1] * updated, axis=0, keepdims=True)
        )
    readout = jnp.concatenate(readout, axis=0)
    normed = (
        readout
        * lax.rsqrt(jnp.mean(readout * readout, axis=1, keepdims=True) + 1e-05)
        * out_gain[...].astype(F32)
    )
    gated = (normed * (outgate * jax.nn.sigmoid(outgate))).astype(BF16)
    for t in range(n):
        mix_send[t] = jnp.dot(
            gated, wout[:, t * WIDTH : (t + 1) * WIDTH], preferred_element_type=F32
        ).astype(BF16)
    for d in range(1, n):
        to = up(tp, d)
        send(mix_send.at[to], mix_recv.at[d], m_send, m_recv, at(z, y, to))
    store_state = pltpu.make_async_copy(state, state_out_hbm, load_sem.at[18])
    store_state.start()
    with jax.named_scope("mixed"):
        mixed = mix_send[tp].astype(F32)
        through(mix_recv.at[1:n], m_recv)
        for d in range(1, n):
            mixed += mix_recv[d].astype(F32)
        second = (first.astype(F32) + mixed).astype(BF16)
        mid[...] = second

    with jax.named_scope("gather2"):
        spread(1, mid)
        gather(1)
    with jax.named_scope("take2"):
        take_weights(0, 1)
        take_weights(1, 1)
    with jax.named_scope("gathered2"):
        gathered(1)
    with jax.named_scope("inner2"):
        units = inner_units(1)
    with jax.named_scope("scatter2"):
        scatter(1, units)
    with jax.named_scope("reduce2"):
        reduce(1)
    with jax.named_scope("reduced2"):
        last[...] = (second.astype(F32) + 0.5 * reduced(1)).astype(BF16)
    store = pltpu.make_async_copy(last, hidden_out_hbm, load_sem.at[19])
    store.start()
    with jax.named_scope("sent"):
        through(gains.at[1:n], gain_send)
        through(rows_in.at[1:n], x_send)
        through(mix_recv.at[1:n], m_send)
        for f in range(2):
            for kind in range(2):
                weights_sent(kind, f)
            for half, red in ((0, red0), (1, red1)):
                through(red.at[f, 1:n], b_send.at[f, half])
                through(red.at[f, 1:n], c_send.at[f, half])
                through(sum0.at[f, 1:n], a_send.at[f, half])
                through(sum0.at[f, 1:n], d_send.at[f, half])

        @pl.when(jnp.logical_not(home))
        def _():
            for f in range(2):
                for half in range(2):
                    through(sum0.at[f, 0], a_send.at[f, half])
                    through(sum0.at[f, 0], d_send.at[f, half])

    store_state.wait()
    store.wait()


def hand_over(hidden_hbm, state_hbm, hidden_out_hbm, state_out_hbm, hid, state, in_sem, out_sem):
    rows = ROWS // PIECES
    parts = [(hidden_hbm, hid, hidden_out_hbm)]
    for i in range(PIECES):
        part = pl.ds(i * rows, rows)
        parts.append((state_hbm.at[part], state.at[part], state_out_hbm.at[part]))
    ins = [pltpu.make_async_copy(a, b, in_sem.at[i]) for i, (a, b, _) in enumerate(parts)]
    outs = [pltpu.make_async_copy(b, c, out_sem.at[i]) for i, (_, b, c) in enumerate(parts)]
    for copy in ins:
        copy.start()
    for copy, onward in zip(ins, outs):
        copy.wait()
        onward.start()
    for onward in outs:
        onward.wait()


def layer(
    hidden_in,
    first_gain,
    first_gate_proj,
    first_up_proj,
    first_down_proj,
    mix_gain,
    query_weight,
    forget_weight,
    input_weight,
    outgate_weight,
    forget_floor,
    state_in,
    out_gain,
    mix_out_weight,
    second_gain,
    second_gate_proj,
    second_up_proj,
    second_down_proj,
):
    n = lax.axis_size("tp")
    assert lax.axis_size("kv") == n * n
    state_shape = (ROWS, HEAD, HEAD)
    dma = pltpu.SemaphoreType.DMA
    vmem = pltpu.VMEM
    any_space = pl.BlockSpec(memory_space=pl.ANY)
    hidden_out, state_out = pl.pallas_call(
        functools.partial(kernel, n),
        out_shape=(
            jax.ShapeDtypeStruct((ROWS, WIDTH), BF16),
            jax.ShapeDtypeStruct(state_shape, F32),
        ),
        in_specs=[any_space] * 18,
        out_specs=(any_space, any_space),
        scratch_shapes=[
            vmem((ROWS, WIDTH), BF16),
            vmem((2 * n, HALF), BF16),
            vmem((2, 2, HALF), BF16),
            vmem((1, HEAD), F32),
            vmem((1, HEAD), BF16),
            vmem((n, 8, HALF), F32),
            vmem((2, n, 3, HID, WIDTH), BF16),
            vmem((n * WIDTH, 4 * HEAD), BF16),
            vmem((HEAD, n * WIDTH), BF16),
            vmem(state_shape, F32),
            vmem((2, n, n * ROWS, WIDTH), BF16),
            vmem((2, n, n * ROWS, WIDTH), BF16),
            vmem((2, n, n, ROWS, HALF), BF16),
            vmem((2, n, n, ROWS, HALF), BF16),
            vmem((2, n, ROWS, HALF), BF16),
            vmem((2, n, ROWS, HALF), BF16),
            vmem((2, n, ROWS, HALF), BF16),
            vmem((2, n, ROWS, HALF), BF16),
            vmem((ROWS, WIDTH), BF16),
            vmem((n, ROWS, WIDTH), BF16),
            vmem((n, ROWS, WIDTH), BF16),
            vmem((n, ROWS, WIDTH), BF16),
            vmem((ROWS, WIDTH), BF16),
            dma((20,)),
            dma,
            dma,
            dma((2, 2)),
            dma((2, 2)),
            dma((2, 2)),
            dma((2, 2)),
            dma((2, 2)),
            dma((2, 2)),
            dma((2, 2)),
            dma((2, 2)),
            dma((2, 2)),
            dma((2, 2)),
            dma((2, 2)),
            dma((2, 2)),
            dma,
            dma,
            dma,
            dma,
        ],
        compiler_params=pltpu.CompilerParams(
            collective_id=0, has_side_effects=True, vmem_limit_bytes=60 * 1024 * 1024
        ),
        name="layer",
    )(
        hidden_in,
        mix_gain.reshape(2 * n, HALF),
        first_gain.reshape(2, HALF),
        second_gain.reshape(2, HALF),
        forget_floor.reshape(1, HEAD),
        out_gain.reshape(1, HEAD),
        first_gate_proj.T,
        first_up_proj.T,
        first_down_proj,
        second_gate_proj.T,
        second_up_proj.T,
        second_down_proj,
        query_weight,
        forget_weight,
        input_weight,
        outgate_weight,
        mix_out_weight,
        state_in.reshape(state_shape),
    )
    hidden_out, state_out = pl.pallas_call(
        hand_over,
        out_shape=(
            jax.ShapeDtypeStruct((ROWS, WIDTH), BF16),
            jax.ShapeDtypeStruct(state_shape, F32),
        ),
        in_specs=[any_space] * 2,
        out_specs=(any_space, any_space),
        scratch_shapes=[
            vmem((ROWS, WIDTH), BF16),
            vmem(state_shape, F32),
            dma((PIECES + 1,)),
            dma((PIECES + 1,)),
        ],
        compiler_params=pltpu.CompilerParams(vmem_limit_bytes=60 * 1024 * 1024),
        name="hand_over",
    )(hidden_out, state_out)
    return hidden_out, state_out.reshape(ROWS, 1, HEAD, HEAD)


def solution(mesh):
    placed = (
        P("kv", "tp"),
        P("tp"),
        P("tp", "kv"),
        P("tp", "kv"),
        P("kv", "tp"),
        P(),
        P(None, "tp"),
        P(None, "tp"),
        P(None, "tp"),
        P(None, "tp"),
        P("tp"),
        P("kv", "tp", None, None),
        P("tp"),
        P("tp", None),
        P("tp"),
        P("tp", "kv"),
        P("tp", "kv"),
        P("kv", "tp"),
    )
    return jax.shard_map(
        layer,
        mesh=mesh,
        in_specs=placed,
        out_specs=(P("kv", "tp"), P("kv", "tp", None, None)),
        check_vma=False,
    )
```

time: 90.7 us -> 82.4 us (0.908)
  local copies, waits for them, and re-layouts: 7.44 us -> 0 us
  Pallas kernels: 82 us -> 81 us
    unnamed x12 -> x0, local copies, waits for them, and re-layouts: 6.22 us -> none
    pallas_call x1, Pallas kernels: 82 us -> 79 us  [layer(): pl.pallas_call(functools.partial(kernel, n), out_shape=(jax.ShapeDtypeStr...]
    pallas_call x0 -> x1, Pallas kernels: none -> 2.01 us  [layer(): pl.pallas_call(hand_over, out_shape=(jax.ShapeDtypeStruct((ROWS, WIDTH),...]
    concatenate x1 -> x0, local copies, waits for them, and re-layouts: 1.21 us -> none  [layer(): jnp.concatenate([jnp.pad(mix_gain.astype(F32).reshape(n, WIDTH), ((0, 8 -...]
where the time goes in v2:
time: 82.4 us; the launch traced here: 81.7 us
  Pallas kernels  81 us (98%)
    pallas_call x1, Pallas kernels, layer(): pl.pallas_call(functools.partial(kernel, n), out_shape=(jax.ShapeDtypeStr...  79 us
    pallas_call x1, Pallas kernels, layer(): pl.pallas_call(hand_over, out_shape=(jax.ShapeDtypeStruct((ROWS, WIDTH),...  2.01 us

profile of v2, /device:TPU:1, one launch (start us, length us, event | category | flops | bytes accessed | tf_op | source)
XLA Modules:
  0.0 81.7 jit_solution(4871294355954854128)
XLA Ops:
  0.6 79.0 %layer.1 = (bf16[16,256]{1,0:T(8,128)(2,1)}, f32[16,128,128]{2,1,0:T(8,128)}) custom-call(bf16[16,256]{1,0:T(8,128)(2,1)} %hidden_hbm.1, bf16[16,128]{1,0:T(8,128)(2,1)} %bitcast.18, bf16[2,128]{1,0:T(2,128)(2,1)} %bitcast.19, bf16[2,128]{1,0:T(2,128)(2,1)} %bitcast.20, f32[1,128]{1,0:T(1,128)} %bitcast.21, bf16[1,128]{1,0:T(2,128)(2,1)} %bitcast.22, ...), custom_call_target="tpu_custom_call" | custom-call | tf_op jit(solution)/shard_map/layer/pallas_call | solution.py:498
  79.6 2.0 %hand_over.1 = (bf16[16,256]{1,0:T(8,128)(2,1)}, f32[16,128,128]{2,1,0:T(8,128)}) custom-call(bf16[16,256]{1,0:T(8,128)(2,1)} %get-tuple-element.6.hidden_hbm, f32[16,128,128]{2,1,0:T(8,128)} %get-tuple-element.7.state_hbm), custom_call_target="tpu_custom_call" | custom-call | tf_op jit(solution)/shard_map/hand_over/pallas_call | solution.py:574
